TPU v7x, 32 devices: a whole 2x2x4 slice. The times are simulated.
32 devices in a mesh: ep: 8 (over z, core), tp: 4 (over y, x).
Axes of the slice: x: 2, y: 2, z: 4, core: 2. Of those that a mesh axis runs over, the one named last changes fastest.
Arguments:
- q_latent: bfloat16 [1536, 512], P('ep'), may hold values from -6 to 6
- kv_latent: bfloat16 [1536, 256], P('ep'), may hold values from -6 to 6
- rope_key: bfloat16 [1536, 64], P('ep'), may hold values from -900 to 900
- q_gain: float32 [512], replicated, may hold values from 0.1 to 1.9
- kv_gain: float32 [256], replicated, may hold values from 0.1 to 1.9
- w_query: bfloat16 [512, 3072], P(None, 'tp'), may hold values from -0.25 to 0.25
- w_key: bfloat16 [256, 2048], P(None, 'tp'), may hold values from -0.375 to 0.375
- w_value: bfloat16 [256, 2048], P(None, 'tp'), may hold values from -0.375 to 0.375
- w_mix_out: bfloat16 [2048, 2048], P('tp'), may hold values from -0.125 to 0.125
- expert_in: bfloat16 [1024, 2048], P('ep'), may hold values from -6 to 6
- norm_gain: float32 [2048], replicated, may hold values from 0.1 to 1.9
- routes: int32 [1024, 2], P('ep'), may hold values from 0 to 7, all different within a row; in each aligned block of 128 rows (0 to 127, 128 to 255, ...) at most 64 rows name the same one
- route_scores: float32 [1024, 2], P('ep'), may hold values from 0.05 to 1
- w_gate: bfloat16 [8, 2048, 4096], P('ep', None, 'tp'), may hold values from -0.125 to 0.125
- w_up: bfloat16 [8, 2048, 4096], P('ep', None, 'tp'), may hold values from -0.125 to 0.125
- w_down: bfloat16 [8, 4096, 2048], P('ep', 'tp'), may hold values from -0.125 to 0.125
Outputs:
- mixed: bfloat16 [1536, 2048], P(('ep', 'tp'))
- expert_out: bfloat16 [1024, 2048], P('ep', 'tp')
Inputs may be any that keep to these rules, and one draw needn't show every extreme that they name: `routes`: each row names 2 different experts; in the rows of one index of ep no expert is named by more than 64 rows, a bound that some block reaches.
All inputs are finite; a program needn't handle non-finite values.
Results may differ from a plain program's by a relative error of at most 0.03.
The roundings to bfloat16 on the way count: a program that leaves them out, or rounds other values in their place, can miss the bound.
Values may be sent and summed in bfloat16 or wider, within the bound.
No kernel may reach another device: no remote copies, remote signals or barrier semaphores. Data moves between devices by JAX's collectives and lax.ppermute only.
A program may use at most 64 MiB of HBM per device.

v0:
```python
import jax
import jax.numpy as jnp
from jax import lax
from jax.sharding import PartitionSpec as P

NOPE = 128
ROPE = 64
VDIM = 128
eps_norm = 1e-05
rope_base = 10000.0


def rms_scale(values, gain):
    wide = values.astype(jnp.float32)
    return wide * lax.rsqrt(jnp.mean(wide * wide, -1, keepdims=True) + eps_norm) * gain


def rotate(values, cosine, sine):
    first, second = jnp.split(values, 2, axis=-1)
    return jnp.concatenate([first * cosine - second * sine, first * sine + second * cosine], -1)


def angles(positions):
    inverse = rope_base ** (-jnp.arange(0, ROPE, 2).astype(jnp.float32) / ROPE)
    phase = positions[:, None] * inverse[None, :]
    return (jnp.cos(phase), jnp.sin(phase))


def mixer(q_latent, kv_latent, rope_key, q_gain, kv_gain, w_query, w_key, w_value, w_mix_out):
    token_count = q_latent.shape[0]
    head_count = w_key.shape[1] // NOPE
    offset = lax.axis_index("ep") * token_count
    positions = (offset + jnp.arange(token_count, dtype=jnp.int32)).astype(jnp.float32)
    cosine, sine = angles(positions)
    q_normed = rms_scale(q_latent, q_gain).astype(jnp.bfloat16)
    kv_normed = rms_scale(kv_latent, kv_gain).astype(jnp.bfloat16)
    key_turned = rotate(rope_key.astype(jnp.float32), cosine, sine).astype(jnp.bfloat16)
    query = jnp.dot(q_normed, w_query, preferred_element_type=jnp.float32).astype(jnp.bfloat16)
    query = query.reshape(token_count, head_count, NOPE + ROPE)
    q_pass = query[:, :, :NOPE]
    q_turned = rotate(
        query[:, :, NOPE:].astype(jnp.float32), cosine[:, None, :], sine[:, None, :]
    ).astype(jnp.bfloat16)
    factor = (NOPE + ROPE) ** (-0.5)
    peak = jnp.full((head_count, token_count), -jnp.inf, jnp.float32)
    total = jnp.zeros((head_count, token_count), jnp.float32)
    summed = jnp.zeros((token_count, head_count, VDIM), jnp.float32)
    latent = lax.all_gather(kv_normed, "ep", axis=0, tiled=True)
    turned = lax.all_gather(key_turned, "ep", axis=0, tiled=True)
    count = latent.shape[0]
    keys = jnp.dot(latent, w_key, preferred_element_type=jnp.float32).astype(jnp.bfloat16)
    keys = keys.reshape(count, head_count, NOPE)
    values = jnp.dot(latent, w_value, preferred_element_type=jnp.float32).astype(jnp.bfloat16)
    values = values.reshape(count, head_count, VDIM)
    scores = jnp.einsum("qhd,khd->hqk", q_pass, keys, preferred_element_type=jnp.float32)
    scores = (
        scores + jnp.einsum("qhd,kd->hqk", q_turned, turned, preferred_element_type=jnp.float32)
    ) * factor
    fresh = jnp.max(scores, -1)
    fade = jnp.exp(peak - fresh)
    weights = jnp.exp(scores - fresh[:, :, None])
    total = total * fade + jnp.sum(weights, -1)
    update = jnp.einsum(
        "hqk,khd->qhd", weights.astype(jnp.bfloat16), values, preferred_element_type=jnp.float32
    )
    summed = summed * jnp.transpose(fade)[:, :, None] + update
    peak, total, summed = (fresh, total, summed)
    attended = (summed / jnp.transpose(total)[:, :, None]).astype(jnp.bfloat16)
    attended = attended.reshape(token_count, head_count * VDIM)
    return lax.psum_scatter(
        jnp.dot(attended, w_mix_out, preferred_element_type=jnp.float32).astype(jnp.bfloat16),
        "tp",
        scatter_dimension=0,
        tiled=True,
    )


def experts(expert_in, norm_gain, routes, route_scores, w_gate, w_up, w_down):
    token_count, width = expert_in.shape
    choose = routes.shape[1]
    expert_count = lax.axis_size("ep")
    slots = 2 * choose * token_count // expert_count
    wide = expert_in.astype(jnp.float32)
    centered = wide - jnp.mean(wide, -1, keepdims=True)
    normed = (
        centered
        * lax.rsqrt(jnp.mean(centered * centered, -1, keepdims=True) + eps_norm)
        * norm_gain
    ).astype(jnp.bfloat16)
    shares = route_scores / jnp.sum(route_scores, -1, keepdims=True)
    flat_expert = routes.reshape(-1)
    onehot = (flat_expert[:, None] == jnp.arange(expert_count, dtype=jnp.int32)[None, :]).astype(
        jnp.int32
    )
    before = jnp.sum((jnp.cumsum(onehot, 0) - onehot) * onehot, 1)
    target = flat_expert * slots + before
    source = jnp.arange(token_count * choose, dtype=jnp.int32) // choose
    table = jnp.full((expert_count * slots,), token_count, jnp.int32).at[target].set(source)
    padded = jnp.concatenate([normed, jnp.zeros((1, width), jnp.bfloat16)], 0)
    outgoing = padded[table].reshape(expert_count, slots, width)
    gate_weight = w_gate[0]
    up_weight = w_up[0]
    down_weight = w_down[0]
    arrived = lax.all_to_all(outgoing, "ep", split_axis=0, concat_axis=0, tiled=True).reshape(
        expert_count * slots, width
    )
    gate = jnp.dot(arrived, gate_weight, preferred_element_type=jnp.float32)
    up = jnp.dot(arrived, up_weight, preferred_element_type=jnp.float32)
    hidden = (jax.nn.silu(gate) * up).astype(jnp.bfloat16)
    summed = lax.psum_scatter(
        lax.dot_general(
            down_weight, hidden, (((0,), (1,)), ((), ())), preferred_element_type=jnp.float32
        ).astype(jnp.bfloat16),
        "tp",
        scatter_dimension=0,
        tiled=True,
    )
    feature_count = summed.shape[0]
    returned = lax.all_to_all(
        summed.reshape(feature_count, expert_count, slots),
        "ep",
        split_axis=1,
        concat_axis=1,
        tiled=True,
    )
    picked = jnp.take(returned.reshape(feature_count, expert_count * slots), target, axis=1)
    picked = picked.reshape(feature_count, token_count, choose).astype(jnp.float32)
    combined = jnp.sum(picked * shares[None, :, :], -1)
    return jnp.transpose(combined).astype(jnp.bfloat16)


def body(
    q_latent,
    kv_latent,
    rope_key,
    q_gain,
    kv_gain,
    w_query,
    w_key,
    w_value,
    w_mix_out,
    expert_in,
    norm_gain,
    routes,
    route_scores,
    w_gate,
    w_up,
    w_down,
):
    mixed = mixer(
        q_latent, kv_latent, rope_key, q_gain, kv_gain, w_query, w_key, w_value, w_mix_out
    )
    expert_out = experts(expert_in, norm_gain, routes, route_scores, w_gate, w_up, w_down)
    return (mixed, expert_out)


def solution(mesh):
    in_specs = (
        P("ep", None),
        P("ep", None),
        P("ep", None),
        P(),
        P(),
        P(None, "tp"),
        P(None, "tp"),
        P(None, "tp"),
        P("tp", None),
        P("ep", None),
        P(),
        P("ep", None),
        P("ep", None),
        P("ep", None, "tp"),
        P("ep", None, "tp"),
        P("ep", "tp", None),
    )
    out_specs = (P(("ep", "tp"), None), P("ep", "tp"))
    return jax.shard_map(body, mesh=mesh, in_specs=in_specs, out_specs=out_specs, check_vma=False)
```

profile of v0, /device:TPU:0, one launch (start us, length us, event | category | flops | bytes accessed | tf_op | source)
XLA Modules:
  0.0 162.9 jit_solution(18064462734204936463)
XLA Ops:
  7.2 0.0 copy-start
  7.2 0.9 copy.51
  8.1 0.1 eq.26
  8.3 0.1 reshape.190
  8.4 0.7 broadcast_multiply_fusion
  9.1 0.6 reduce-window.6
  9.7 0.2 slice_reduce_fusion
  9.9 0.1 copy.55
  10.0 0.1 mul.215
  10.2 0.1 fusion.59
  10.3 1.4 scatter_custom_fusion
  11.7 1.2 convert_reduce_fusion
  12.9 1.3 fusion.37
  14.3 1.4 fusion.39
  15.7 3.3 %gather_fusion = bf16[512,2048]{1,0:T(8,128)(2,1)} fusion(bf16[129,2048]{1,0:T(8,128)(2,1)S(1)} %concatenate.13, s32[1024]{0:T(1024)S(1)} %pad_clamp_fusion.1), kind=kCustom, calls=%fused_computation | custom fusion | bytes 4196352 | tf_op jit(solution)/shard_map/gather | solution.py:100
  19.1 6.5 %all-to-all-start = ((bf16[8,64,2048]{2,1,0:T(8,128)(2,1)}), bf16[8,64,2048]{2,1,0:T(8,128)(2,1)}, u32[]{:S(2)}, u32[]{:S(2)}) async-start(bf16[8,64,2048]{2,1,0:T(8,128)(2,1)} %bitcast.82), calls=%async_computation.1 | async-start | bytes 4194304 | tf_op jit(solution)/shard_map/all_to_all | solution.py:104
  25.6 0.0 reduce-scatter.5.cloned.1.call-start
  25.6 0.0 copy-done.5
  25.7 0.1 fusion.42
  25.8 0.2 multiply_cosine_fusion
  26.1 1.5 convolution_convert_fusion.3
  27.6 47.2 %all-to-all-done = bf16[8,64,2048]{2,1,0:T(8,128)(2,1)} async-done(((bf16[8,64,2048]{2,1,0:T(8,128)(2,1)}), bf16[8,64,2048]{2,1,0:T(8,128)(2,1)}, u32[]{:S(2)}, u32[]{:S(2)}) %all-to-all-start) | async-done | bytes 2097184 | tf_op jit(solution)/shard_map/all_to_all | solution.py:104
  74.7 6.5 %fusion.5 = f32[512,1024]{1,0:T(8,128)} fusion(bf16[512,2048]{1,0:T(8,128)(2,1)} %bitcast.12, bf16[1,2048,1024]{2,1,0:T(8,128)(2,1)} %param.29), kind=kOutput, calls=%fused_computation.10 | convolution fusion | flops 2147483648 | bytes 8388608 | tf_op jit(solution)/shard_map/dot_general | solution.py:107
  81.2 10.6 %fusion.12 = bf16[2048,512]{0,1:T(8,128)(2,1)} fusion(bf16[1,1024,2048]{2,1,0:T(8,128)(2,1)} %param.31, f32[512,1024]{1,0:T(8,128)} %fusion.5, bf16[512,2048]{1,0:T(8,128)(2,1)} %bitcast.12, bf16[1,2048,1024]{2,1,0:T(8,128)(2,1)} %param.30), kind=kOutput, calls=%fused_computation.17 | convolution fusion | flops 4299161600 | bytes 14680064 | tf_op jit(solution)/shard_map/dot_general | solution.py:111
  91.8 0.0 reduce-scatter.5.cloned.1.call-update
  91.8 0.0 copy-start.3
  91.8 0.0 copy-start.9
  91.8 0.0 reduce-scatter.3.cloned.1.call-start
  91.9 0.4 reshape.186
  92.3 0.1 slice.21
  92.4 0.1 copy.60
  92.5 14.2 %all-gather = bf16[8,192,64]{1,2,0:T(8,128)(2,1)S(1)} all-gather(bf16[1,192,64]{1,2,0:T(8,128)(2,1)S(1)} %maximum_bitcast_fusion), channel_id=1, replica_groups=mesh['ep'=8,'tp'=4] {'ep'}, dimensions={0}, use_global_device_ids=true | all-gather | bytes 221184 | tf_op jit(solution)/shard_map/all_gather | solution.py:49
  106.7 0.1 copy.47
  106.9 0.2 reshape.223
  107.1 0.0 copy-done.3
  107.1 0.1 fusion.45
  107.3 0.0 copy-done.9
  107.3 0.1 fusion.47
  107.4 16.3 %all_gather.6 = bf16[1536,256]{1,0:T(8,128)(2,1)S(1)} all-gather(bf16[192,256]{1,0:T(8,128)(2,1)S(1)} %fusion.47), channel_id=1, replica_groups=mesh['ep'=8,'tp'=4] {'ep'}, dimensions={0}, use_global_device_ids=true | all-gather | bytes 884736 | tf_op jit(solution)/shard_map/all_gather | solution.py:48
  123.7 1.6 convolution_convert_fusion.1
  125.3 0.0 slice-start
  125.3 0.8 fusion.54
  126.1 0.1 slice-done
  126.2 0.9 fusion.65
  127.1 0.0 copy-start.4
  127.1 0.8 fusion.7
  127.9 0.2 copy-done.4
  128.0 0.6 convolution_convert_fusion
  128.7 0.9 fusion.34
  129.6 0.0 copy-start.6
  129.6 0.0 copy-start.7
  129.6 1.5 convolution_convert_fusion.2
  131.1 0.0 reduce-scatter.3.cloned.1.call-update
  131.2 0.0 reduce-scatter.5.cloned.1.call-done
  131.2 3.5 %all-to-all-start.1 = ((bf16[512,8,64]{0,2,1:T(8,128)(2,1)}), bf16[512,8,64]{0,2,1:T(8,128)(2,1)S(1)}, u32[]{:S(2)}, u32[]{:S(2)}) async-start(bf16[512,8,64]{0,2,1:T(8,128)(2,1)} %bitcast.86), calls=%async_computation.3 | async-start | bytes 1048576 | tf_op jit(solution)/shard_map/all_to_all | solution.py:119
  134.7 0.1 reduce_sum.83
  134.8 0.1 copy.53
  134.9 0.1 copy.54
  135.1 0.1 copy.56
  135.2 14.7 %all-to-all-done.1 = bf16[512,8,64]{0,2,1:T(8,128)(2,1)S(1)} async-done(((bf16[512,8,64]{0,2,1:T(8,128)(2,1)}), bf16[512,8,64]{0,2,1:T(8,128)(2,1)S(1)}, u32[]{:S(2)}, u32[]{:S(2)}) %all-to-all-start.1) | async-done | bytes 524320 | tf_op jit(solution)/shard_map/all_to_all | solution.py:119
  149.9 1.2 gather_fusion.1
  151.1 0.1 gather.11
  151.2 1.5 multiply_reduce_fusion
  152.7 3.4 %reduce-scatter.3.cloned.1.call-done = bf16[48,2048]{1,0:T(8,128)(2,1)} async-done(((bf16[192,2048]{1,0:T(8,128)(2,1)}), bf16[48,2048]{1,0:T(8,128)(2,1)}) %reduce-scatter.3.cloned.1.call-update) | async-done | bytes 196624 | tf_op jit(solution)/shard_map/reduce_scatter | solution.py:70
  (34 shorter events, 0.3 us)
Async XLA Ops:
  7.2 122.4 %copy-start = (bf16[512,2048]{1,0:T(8,128)(2,1)S(1)}, bf16[512,2048]{1,0:T(8,128)(2,1)}, u32[]{:S(2)}) copy-start(bf16[512,2048]{1,0:T(8,128)(2,1)} %param.24) | copy-start | bytes 6291460
  19.1 6.5 %copy-start.5 = (bf16[192,64]{0,1:T(8,128)(2,1)S(1)}, bf16[192,64]{0,1:T(8,128)(2,1)}, u32[]{:S(2)}) copy-start(bf16[192,64]{0,1:T(8,128)(2,1)} %param.18) | copy-start | bytes 73732
  19.1 6.6 %copy-start.2 = (bf16[192,512]{1,0:T(8,128)(2,1)S(1)}, bf16[192,512]{1,0:T(8,128)(2,1)}, u32[]{:S(2)}) copy-start(bf16[192,512]{1,0:T(8,128)(2,1)} %param.16) | copy-start | bytes 589828
  19.1 7.0 %copy-start.8 = (f32[512]{0:T(512)S(1)}, f32[512]{0:T(512)}, u32[]{:S(2)}) copy-start(f32[512]{0:T(512)} %param.19) | copy-start | bytes 6148
  19.1 55.6 %all-to-all-start = ((bf16[8,64,2048]{2,1,0:T(8,128)(2,1)}), bf16[8,64,2048]{2,1,0:T(8,128)(2,1)}, u32[]{:S(2)}, u32[]{:S(2)}) async-start(bf16[8,64,2048]{2,1,0:T(8,128)(2,1)} %bitcast.82), calls=%async_computation.1 | async-start | bytes 4194304 | tf_op jit(solution)/shard_map/all_to_all | solution.py:104
  25.6 105.6 %reduce-scatter.5.cloned.1.call-start = ((), (), s32[]{:S(2)}) async-start(), calls=%async_computation.5 | async-start | bytes 2621440 | tf_op jit(solution)/shard_map/reduce_scatter | solution.py:110
  91.8 15.3 %copy-start.3 = (bf16[192,256]{1,0:T(8,128)(2,1)S(1)}, bf16[192,256]{1,0:T(8,128)(2,1)}, u32[]{:S(2)}) copy-start(bf16[192,256]{1,0:T(8,128)(2,1)} %param.17) | copy-start | bytes 294916
  91.8 15.5 %copy-start.9 = (f32[256]{0:T(256)S(1)}, f32[256]{0:T(256)}, u32[]{:S(2)}) copy-start(f32[256]{0:T(256)} %param.20) | copy-start | bytes 3076
  91.8 64.3 %reduce-scatter.3.cloned.1.call-start = ((), (), s32[]{:S(2)}) async-start(), calls=%async_computation.4 | async-start | bytes 983040 | tf_op jit(solution)/shard_map/reduce_scatter | solution.py:70
  92.3 31.4 %copy-start.1 = (bf16[192,4,192]{2,1,0:T(4,128)(2,1)}, bf16[192,4,192]{2,1,0:T(4,128)(2,1)S(1)}, u32[]{:S(2)}) copy-start(bf16[192,4,192]{2,1,0:T(4,128)(2,1)S(1)} %reshape.186) | copy-start | bytes 884740
  125.3 0.9 slice-start
  127.1 1.0 copy-start.4
  129.6 5.3 %copy-start.6 = (s32[128,2]{0,1:T(2,128)S(1)}, s32[128,2]{0,1:T(2,128)}, u32[]{:S(2)}) copy-start(s32[128,2]{0,1:T(2,128)} %param.27) | copy-start | bytes 3076
  129.6 5.5 %copy-start.7 = (f32[128,2]{0,1:T(2,128)S(1)}, f32[128,2]{0,1:T(2,128)}, u32[]{:S(2)}) copy-start(f32[128,2]{0,1:T(2,128)} %param.28) | copy-start | bytes 3076
  131.2 18.8 %all-to-all-start.1 = ((bf16[512,8,64]{0,2,1:T(8,128)(2,1)}), bf16[512,8,64]{0,2,1:T(8,128)(2,1)S(1)}, u32[]{:S(2)}, u32[]{:S(2)}) async-start(bf16[512,8,64]{0,2,1:T(8,128)(2,1)} %bitcast.86), calls=%async_computation.3 | async-start | bytes 1048576 | tf_op jit(solution)/shard_map/all_to_all | solution.py:119
Sparse Core Ops, SparseCore 0:
  91.9 34.1 reduce-scatter.4
  131.3 24.7 reduce-scatter.2
where the time goes:
time: 164 us; the launch traced here: 163 us
  waiting for transfers between devices  65.3 us (40%)
  blocking collectives  30.5 us (19%)
  matrix products  24.9 us (15%)
  between operations  14.4 us (9%)
  starting transfers between devices  10.1 us (6%)
  local copies, waits for them, and re-layouts  9.44 us (6%)
  other arithmetic  8.38 us (5%)
    all_to_all x1, waiting for transfers between devices, experts(): lax.all_to_all(outgoing, 'ep', split_axis=0, concat_axis=0, tiled=True)  47.2 us
    all_gather x1, blocking collectives, mixer(): latent = lax.all_gather(kv_normed, 'ep', axis=0, tiled=True)  16.3 us
    all_to_all x1, waiting for transfers between devices, experts(): lax.all_to_all(summed.reshape(feature_count, expert_count, slots), 'ep',...  14.7 us
    all_gather x1, blocking collectives, mixer(): turned = lax.all_gather(key_turned, 'ep', axis=0, tiled=True)  14.2 us
    dot_general x1, matrix products, experts(): lax.dot_general(down_weight, hidden, (((0,), (1,)), ((), ())), preferred_...  10.6 us
    all_to_all x1, starting transfers between devices, experts(): lax.all_to_all(outgoing, 'ep', split_axis=0, concat_axis=0, tiled=True)  6.49 us
    dot_general x1, matrix products, experts(): gate = jnp.dot(arrived, gate_weight, preferred_element_type=jnp.float32)  6.48 us
    all_to_all x1, starting transfers between devices, experts(): lax.all_to_all(summed.reshape(feature_count, expert_count, slots), 'ep',...  3.5 us
  transfers between devices with their start and end apart: 4, of which 3 were waited for; matrix products, arithmetic and copies ran while one was open for 8% of the time, Pallas kernels for 0%

commit v1 on v0

--- a/solution.py
+++ b/solution.py
@@ -116,13 +116,10 @@
         tiled=True,
     )
     feature_count = summed.shape[0]
-    returned = lax.all_to_all(
-        summed.reshape(feature_count, expert_count, slots),
-        "ep",
-        split_axis=1,
-        concat_axis=1,
-        tiled=True,
-    )
+    own = summed.reshape(feature_count, expert_count, slots)
+    parts = jnp.split(own, lax.axis_size("ep"), axis=1)
+    received = lax.all_to_all(jnp.stack(parts), "ep", 0, 0)
+    returned = jnp.concatenate(received, axis=1)
     picked = jnp.take(returned.reshape(feature_count, expert_count * slots), target, axis=1)
     picked = picked.reshape(feature_count, token_count, choose).astype(jnp.float32)
     combined = jnp.sum(picked * shares[None, :, :], -1)

time: 164 us -> 172 us (1.049)
  local copies, waits for them, and re-layouts: 9.44 us -> 21.1 us
  waiting for transfers between devices: 65.3 us -> 61.9 us
    unnamed x23 -> x30, local copies, waits for them, and re-layouts: 1.52 us -> 11.8 us
    reduce_scatter x1, waiting for transfers between devices: 3.37 us -> 0.01 us  [mixer(): lax.psum_scatter(jnp.dot(attended, w_mix_out, preferred_element_type=jnp....]
  transfers between devices with their start and end apart: 4 -> 4, of which waited for: 3 -> 2; matrix products, arithmetic and copies ran while one was open for 8% -> 15% of each run, Pallas kernels for 0% -> 0%
where the time goes in v1:
time: 172 us; the launch traced here: 171 us
  waiting for transfers between devices  61.9 us (36%)
  blocking collectives  30.5 us (18%)
  matrix products  24.9 us (14%)
  local copies, waits for them, and re-layouts  21.1 us (12%)
  between operations  14.4 us (8%)
  starting transfers between devices  10.1 us (6%)
  other arithmetic  8.38 us (5%)
    all_to_all x1, waiting for transfers between devices, experts(): lax.all_to_all(outgoing, 'ep', split_axis=0, concat_axis=0, tiled=True)  47.2 us
    all_gather x1, blocking collectives, mixer(): latent = lax.all_gather(kv_normed, 'ep', axis=0, tiled=True)  16.3 us
    all_to_all x1, waiting for transfers between devices, experts(): received = lax.all_to_all(jnp.stack(parts), 'ep', 0, 0)  14.7 us
    all_gather x1, blocking collectives, mixer(): turned = lax.all_gather(key_turned, 'ep', axis=0, tiled=True)  14.2 us
    unnamed x30, local copies, waits for them, and re-layouts  11.8 us
    dot_general x1, matrix products, experts(): lax.dot_general(down_weight, hidden, (((0,), (1,)), ((), ())), preferred_...  10.6 us
    all_to_all x1, starting transfers between devices, experts(): lax.all_to_all(outgoing, 'ep', split_axis=0, concat_axis=0, tiled=True)  6.49 us
    dot_general x1, matrix products, experts(): gate = jnp.dot(arrived, gate_weight, preferred_element_type=jnp.float32)  6.48 us
  transfers between devices with their start and end apart: 4, of which 2 were waited for; matrix products, arithmetic and copies ran while one was open for 15% of the time, Pallas kernels for 0%

profile of v1, /device:TPU:0, one launch (start us, length us, event | category | flops | bytes accessed | tf_op | source)
XLA Modules:
  0.0 171.2 jit_solution(16169320300648312487)
XLA Ops:
  7.2 0.0 copy-start
  7.2 0.9 copy.51
  8.1 0.1 eq.26
  8.3 0.1 reshape.190
  8.4 0.7 broadcast_multiply_fusion
  9.1 0.6 reduce-window.6
  9.7 0.2 slice_reduce_fusion
  9.9 0.1 copy.55
  10.0 0.1 mul.215
  10.2 0.1 fusion.67
  10.3 1.4 scatter_custom_fusion
  11.7 1.2 convert_reduce_fusion
  12.9 1.3 fusion.37
  14.3 1.4 fusion.39
  15.7 3.3 %gather_fusion = bf16[512,2048]{1,0:T(8,128)(2,1)} fusion(bf16[129,2048]{1,0:T(8,128)(2,1)S(1)} %concatenate.13, s32[1024]{0:T(1024)S(1)} %pad_clamp_fusion.1), kind=kCustom, calls=%fused_computation | custom fusion | bytes 4196352 | tf_op jit(solution)/shard_map/gather | solution.py:100
  19.1 6.5 %all-to-all-start = ((bf16[8,64,2048]{2,1,0:T(8,128)(2,1)}), bf16[8,64,2048]{2,1,0:T(8,128)(2,1)}, u32[]{:S(2)}, u32[]{:S(2)}) async-start(bf16[8,64,2048]{2,1,0:T(8,128)(2,1)} %bitcast.116), calls=%async_computation.1 | async-start | bytes 4194304 | tf_op jit(solution)/shard_map/all_to_all | solution.py:104
  25.6 0.0 reduce-scatter.5.cloned.1.call-start
  25.7 0.1 fusion.42
  25.8 0.2 multiply_cosine_fusion
  26.1 1.5 convolution_convert_fusion.3
  27.6 47.2 %all-to-all-done = bf16[8,64,2048]{2,1,0:T(8,128)(2,1)} async-done(((bf16[8,64,2048]{2,1,0:T(8,128)(2,1)}), bf16[8,64,2048]{2,1,0:T(8,128)(2,1)}, u32[]{:S(2)}, u32[]{:S(2)}) %all-to-all-start) | async-done | bytes 2097184 | tf_op jit(solution)/shard_map/all_to_all | solution.py:104
  74.7 6.5 %fusion.5 = f32[512,1024]{1,0:T(8,128)} fusion(bf16[512,2048]{1,0:T(8,128)(2,1)} %bitcast.12, bf16[1,2048,1024]{2,1,0:T(8,128)(2,1)} %param.29), kind=kOutput, calls=%fused_computation.10 | convolution fusion | flops 2147483648 | bytes 8388608 | tf_op jit(solution)/shard_map/dot_general | solution.py:107
  81.2 10.6 %fusion.12 = bf16[2048,512]{0,1:T(8,128)(2,1)} fusion(bf16[1,1024,2048]{2,1,0:T(8,128)(2,1)} %param.31, f32[512,1024]{1,0:T(8,128)} %fusion.5, bf16[512,2048]{1,0:T(8,128)(2,1)} %bitcast.12, bf16[1,2048,1024]{2,1,0:T(8,128)(2,1)} %param.30), kind=kOutput, calls=%fused_computation.17 | convolution fusion | flops 4299161600 | bytes 14680064 | tf_op jit(solution)/shard_map/dot_general | solution.py:111
  91.8 0.0 reduce-scatter.5.cloned.1.call-update
  91.8 0.0 copy-start.3
  91.8 0.0 copy-start.9
  91.8 0.0 reduce-scatter.3.cloned.1.call-start
  91.9 0.4 reshape.186
  92.3 0.1 slice.21
  92.4 0.1 copy.60
  92.5 14.2 %all-gather = bf16[8,192,64]{1,2,0:T(8,128)(2,1)S(1)} all-gather(bf16[1,192,64]{1,2,0:T(8,128)(2,1)S(1)} %maximum_bitcast_fusion), channel_id=1, replica_groups=mesh['ep'=8,'tp'=4] {'ep'}, dimensions={0}, use_global_device_ids=true | all-gather | bytes 221184 | tf_op jit(solution)/shard_map/all_gather | solution.py:49
  106.7 0.1 copy.47
  106.9 0.2 reshape.223
  107.1 0.1 fusion.45
  107.3 0.1 fusion.47
  107.4 16.3 %all_gather.6 = bf16[1536,256]{1,0:T(8,128)(2,1)S(1)} all-gather(bf16[192,256]{1,0:T(8,128)(2,1)S(1)} %fusion.47), channel_id=1, replica_groups=mesh['ep'=8,'tp'=4] {'ep'}, dimensions={0}, use_global_device_ids=true | all-gather | bytes 884736 | tf_op jit(solution)/shard_map/all_gather | solution.py:48
  123.7 1.6 convolution_convert_fusion.1
  125.3 0.8 fusion.54
  126.1 0.1 slice-done
  126.2 0.9 fusion.73
  127.1 0.8 fusion.7
  127.9 0.2 copy-done.4
  128.0 0.6 convolution_convert_fusion
  128.7 0.9 fusion.34
  129.6 1.5 convolution_convert_fusion.2
  131.1 0.0 reduce-scatter.3.cloned.1.call-update
  131.1 0.0 reduce-scatter.5.cloned.1.call-done
  131.2 1.5 fusion.65
  132.6 1.5 fusion.64
  134.1 1.5 fusion.63
  135.5 1.5 fusion.62
  137.0 1.5 fusion.61
  138.5 1.5 fusion.60
  139.9 1.5 fusion.59
  141.4 1.5 fusion.58
  142.9 3.5 %all-to-all-start.1 = ((bf16[8,512,1,64]{1,3,2,0:T(8,128)(2,1)}), bf16[8,512,1,64]{1,3,2,0:T(8,128)(2,1)S(1)}, u32[]{:S(2)}, u32[]{:S(2)}) async-start(bf16[8,512,1,64]{1,3,2,0:T(8,128)(2,1)} %fusion.58), calls=%async_computation.3 | async-start | bytes 1048576 | tf_op jit(solution)/shard_map/all_to_all | solution.py:121
  146.4 0.1 reduce_sum.83
  146.5 0.1 copy.53
  146.6 0.1 copy.54
  146.8 0.1 copy.56
  146.9 14.7 %all-to-all-done.1 = bf16[8,512,1,64]{1,3,2,0:T(8,128)(2,1)S(1)} async-done(((bf16[8,512,1,64]{1,3,2,0:T(8,128)(2,1)}), bf16[8,512,1,64]{1,3,2,0:T(8,128)(2,1)S(1)}, u32[]{:S(2)}, u32[]{:S(2)}) %all-to-all-start.1) | async-done | bytes 524320 | tf_op jit(solution)/shard_map/all_to_all | solution.py:121
  161.6 1.2 gather_fusion.1
  162.8 0.1 gather.11
  162.9 1.5 multiply_reduce_fusion
  (42 shorter events, 0.3 us)
Async XLA Ops:
  7.2 122.4 %copy-start = (bf16[512,2048]{1,0:T(8,128)(2,1)S(1)}, bf16[512,2048]{1,0:T(8,128)(2,1)}, u32[]{:S(2)}) copy-start(bf16[512,2048]{1,0:T(8,128)(2,1)} %param.24) | copy-start | bytes 6291460
  19.1 6.5 %copy-start.5 = (bf16[192,64]{0,1:T(8,128)(2,1)S(1)}, bf16[192,64]{0,1:T(8,128)(2,1)}, u32[]{:S(2)}) copy-start(bf16[192,64]{0,1:T(8,128)(2,1)} %param.18) | copy-start | bytes 73732
  19.1 6.6 %copy-start.2 = (bf16[192,512]{1,0:T(8,128)(2,1)S(1)}, bf16[192,512]{1,0:T(8,128)(2,1)}, u32[]{:S(2)}) copy-start(bf16[192,512]{1,0:T(8,128)(2,1)} %param.16) | copy-start | bytes 589828
  19.1 7.0 %copy-start.8 = (f32[512]{0:T(512)S(1)}, f32[512]{0:T(512)}, u32[]{:S(2)}) copy-start(f32[512]{0:T(512)} %param.19) | copy-start | bytes 6148
  19.1 55.6 %all-to-all-start = ((bf16[8,64,2048]{2,1,0:T(8,128)(2,1)}), bf16[8,64,2048]{2,1,0:T(8,128)(2,1)}, u32[]{:S(2)}, u32[]{:S(2)}) async-start(bf16[8,64,2048]{2,1,0:T(8,128)(2,1)} %bitcast.116), calls=%async_computation.1 | async-start | bytes 4194304 | tf_op jit(solution)/shard_map/all_to_all | solution.py:104
  25.6 105.6 %reduce-scatter.5.cloned.1.call-start = ((), (), s32[]{:S(2)}) async-start(), calls=%async_computation.5 | async-start | bytes 2621440 | tf_op jit(solution)/shard_map/reduce_scatter | solution.py:110
  91.8 15.3 %copy-start.3 = (bf16[192,256]{1,0:T(8,128)(2,1)S(1)}, bf16[192,256]{1,0:T(8,128)(2,1)}, u32[]{:S(2)}) copy-start(bf16[192,256]{1,0:T(8,128)(2,1)} %param.17) | copy-start | bytes 294916
  91.8 15.5 %copy-start.9 = (f32[256]{0:T(256)S(1)}, f32[256]{0:T(256)}, u32[]{:S(2)}) copy-start(f32[256]{0:T(256)} %param.20) | copy-start | bytes 3076
  91.8 72.6 %reduce-scatter.3.cloned.1.call-start = ((), (), s32[]{:S(2)}) async-start(), calls=%async_computation.4 | async-start | bytes 983040 | tf_op jit(solution)/shard_map/reduce_scatter | solution.py:70
  92.3 31.4 %copy-start.1 = (bf16[192,4,192]{2,1,0:T(4,128)(2,1)}, bf16[192,4,192]{2,1,0:T(4,128)(2,1)S(1)}, u32[]{:S(2)}) copy-start(bf16[192,4,192]{2,1,0:T(4,128)(2,1)S(1)} %reshape.186) | copy-start | bytes 884740
  125.3 0.9 slice-start
  127.1 1.0 copy-start.4
  131.1 15.5 %copy-start.6 = (s32[128,2]{0,1:T(2,128)S(1)}, s32[128,2]{0,1:T(2,128)}, u32[]{:S(2)}) copy-start(s32[128,2]{0,1:T(2,128)} %param.27) | copy-start | bytes 3076
  131.1 15.6 %copy-start.7 = (f32[128,2]{0,1:T(2,128)S(1)}, f32[128,2]{0,1:T(2,128)}, u32[]{:S(2)}) copy-start(f32[128,2]{0,1:T(2,128)} %param.28) | copy-start | bytes 3076
  142.9 18.8 %all-to-all-start.1 = ((bf16[8,512,1,64]{1,3,2,0:T(8,128)(2,1)}), bf16[8,512,1,64]{1,3,2,0:T(8,128)(2,1)S(1)}, u32[]{:S(2)}, u32[]{:S(2)}) async-start(bf16[8,512,1,64]{1,3,2,0:T(8,128)(2,1)} %fusion.58), calls=%async_computation.3 | async-start | bytes 1048576 | tf_op jit(solution)/shard_map/all_to_all | solution.py:121
Sparse Core Ops, SparseCore 0:
  91.9 34.1 reduce-scatter.4
  131.3 24.7 reduce-scatter.2
